TPU v7x, 32 devices: a whole 2x2x4 slice. The times are simulated.
32 devices in a mesh: sp: 4 (over y, x), tp: 8 (over z, core).
Axes of the slice: x: 2, y: 2, z: 4, core: 2. Of those that a mesh axis runs over, the one named last changes fastest.
Arguments:
- queries: bfloat16 [4096, 2048], P('sp', 'tp'), may hold values from -160 to 160
- key_heads: bfloat16 [4096, 512], P('sp'), may hold values from -8 to 8
- value_heads: bfloat16 [4096, 512], P('sp'), may hold values from -4 to 4
- sink_logit: float32 [16], P('tp'), may hold values from -2 to 7
- out_weight: bfloat16 [2048, 2048], P('tp'), may hold values from -0.125 to 0.125
- residual: bfloat16 [4096, 2048], P(('sp', 'tp')), may hold values from -6 to 6
- mixer_gain: float32 [2048], replicated, may hold values from 0.1 to 1.9
- expert_gain: float32 [2048], replicated, may hold values from 0.1 to 1.9
- route_group: int32 [4096], P(('sp', 'tp')), may hold values from 0 to 3, as said below
- route_member: int32 [4096, 2], P(('sp', 'tp')), may hold values from 0 to 2, as said below
- route_weight: bfloat16 [4096, 2], P(('sp', 'tp')), may hold values from 0.19921875 to 1
- gate_weight: bfloat16 [12, 2048, 2048], P('sp', None, 'tp'), may hold values from -0.125 to 0.125
- up_weight: bfloat16 [12, 2048, 2048], P('sp', None, 'tp'), may hold values from -0.125 to 0.125
- down_weight: bfloat16 [12, 2048, 2048], P('sp', 'tp'), may hold values from -0.125 to 0.125
Outputs:
- output: bfloat16 [4096, 2048], P(('sp', 'tp'))
Inputs may be any that keep to these rules, and one draw needn't show every extreme that they name: `route_group`: among the tokens of one device, at most 40 name one group; in every draw one group is named by exactly 40 tokens of every device. `route_member`: the two entries of a token are different members of its group.
All inputs are finite; a program needn't handle non-finite values.
Results may differ from a plain program's by a relative error of at most 0.018.
Values may be sent and summed in bfloat16 or wider, within the bound.
A program may use at most 128 MiB of HBM per device.

v0:
```python
import jax
import jax.numpy as jnp
from jax import lax
from jax.sharding import PartitionSpec as P

HEADS = 16
KV_HEADS = 4
HEAD_DIM = 128
WINDOW = 128
BLOCK = 128
GROUP_EXPERTS = 3
EPS = 1e-06
NEG_BIG = -1e30


def extended(block, sides, width):
    for axis, dim in sides:
        count = lax.axis_size(axis)
        forward = [(i, i + 1) for i in range(count - 1)]
        backward = [(target, source) for source, target in forward]
        low = lax.ppermute(
            lax.slice_in_dim(block, block.shape[dim] - width, None, axis=dim), axis, forward
        )
        high = lax.ppermute(lax.slice_in_dim(block, 0, width, axis=dim), axis, backward)
        block = jnp.concatenate([low, block, high], axis=dim)
    return block


def window_attention(queries, key_heads, value_heads, sink_logit):
    seq_rows = queries.shape[0]
    heads_dev = sink_logit.shape[0]
    key_group = HEADS // KV_HEADS
    key_start = lax.axis_index("tp") * heads_dev // key_group * HEAD_DIM
    key_own = lax.dynamic_slice_in_dim(key_heads, key_start, HEAD_DIM, 1)
    value_own = lax.dynamic_slice_in_dim(value_heads, key_start, HEAD_DIM, 1)
    padded = extended(jnp.stack([key_own, value_own]), (("sp", 1),), WINDOW)
    blocks = seq_rows // BLOCK
    extent = WINDOW // BLOCK
    tile_rows = padded.reshape(2, blocks + 2 * extent, BLOCK, HEAD_DIM)
    key_spans = jnp.concatenate(
        [tile_rows[:, shifted : shifted + blocks] for shifted in range(2 * extent + 1)], axis=2
    )
    offset = lax.axis_index("sp") * seq_rows
    seq_total = seq_rows * lax.axis_size("sp")
    query_pos = offset + jnp.arange(seq_rows, dtype=jnp.int32).reshape(blocks, BLOCK)
    key_pos = (
        offset
        + (jnp.arange(blocks, dtype=jnp.int32) * BLOCK)[:, None]
        + jnp.arange(BLOCK + 2 * WINDOW, dtype=jnp.int32)[None, :]
        - WINDOW
    )
    inside = (
        (jnp.abs(query_pos[:, :, None] - key_pos[:, None, :]) <= WINDOW)
        & (key_pos >= 0)[:, None, :]
        & (key_pos < seq_total)[:, None, :]
    )
    query_blocks = queries.reshape(blocks, BLOCK, heads_dev, HEAD_DIM)
    scores = jnp.einsum(
        "nqhd,nkd->nhqk", query_blocks, key_spans[0], preferred_element_type=jnp.float32
    ) * HEAD_DIM ** (-0.5)
    scores = jnp.where(inside[:, None], scores, NEG_BIG)
    sink_col = sink_logit[None, :, None, None]
    row_top = jnp.maximum(jnp.max(scores, axis=3, keepdims=True), sink_col)
    exp_terms = jnp.exp(scores - row_top)
    row_mass = jnp.sum(exp_terms, axis=3, keepdims=True) + jnp.exp(sink_col - row_top)
    weight = (exp_terms / row_mass).astype(jnp.bfloat16)
    attended = jnp.einsum(
        "nhqk,nkd->nqhd", weight, key_spans[1], preferred_element_type=jnp.float32
    ).astype(jnp.bfloat16)
    return attended.reshape(seq_rows, heads_dev * HEAD_DIM)


def per_device(
    queries,
    key_heads,
    value_heads,
    sink_logit,
    out_weight,
    residual,
    mixer_gain,
    expert_gain,
    route_group,
    route_member,
    route_weight,
    gate_weight,
    up_weight,
    down_weight,
):
    attended = window_attention(queries, key_heads, value_heads, sink_logit)
    tok_rows = residual.shape[0]
    width = out_weight.shape[1]
    projected = lax.psum_scatter(
        jnp.dot(attended, out_weight, preferred_element_type=jnp.float32).astype(jnp.bfloat16),
        "tp",
        scatter_dimension=0,
        tiled=True,
    ).astype(jnp.float32)
    proj_scale = lax.rsqrt(jnp.mean(projected * projected, axis=1, keepdims=True) + EPS)
    mixed_rows = (residual.astype(jnp.float32) + mixer_gain * (projected * proj_scale)).astype(
        jnp.bfloat16
    )
    mixed_float = mixed_rows.astype(jnp.float32)
    norm_scale = lax.rsqrt(jnp.mean(mixed_float * mixed_float, axis=1, keepdims=True) + EPS)
    normed = (mixed_float * norm_scale * expert_gain).astype(jnp.bfloat16)
    groups = lax.axis_size("sp")
    capacity = max(2, (5 * tok_rows + 4 * groups - 1) // (4 * groups))
    group_ids = jnp.arange(groups, dtype=jnp.int32)
    chosen = (route_group[:, None] == group_ids[None, :]).astype(jnp.int32)
    group_rank = jnp.sum(chosen * (jnp.cumsum(chosen, axis=0) - 1), axis=1)
    slot_ids = route_group * capacity + group_rank
    placing = (jnp.arange(groups * capacity, dtype=jnp.int32)[:, None] == slot_ids[None, :]).astype(
        jnp.bfloat16
    )
    member_ids = jnp.arange(GROUP_EXPERTS, dtype=jnp.int32)
    token_gates = jnp.sum(
        route_weight.astype(jnp.float32)[:, :, None]
        * (route_member[:, :, None] == member_ids[None, None, :]).astype(jnp.float32),
        axis=1,
    ).astype(jnp.bfloat16)
    send_rows = (
        jnp.dot(placing, normed, preferred_element_type=jnp.float32)
        .astype(jnp.bfloat16)
        .reshape(groups, capacity, width)
    )
    send_gates = (
        jnp.dot(placing, token_gates, preferred_element_type=jnp.float32)
        .astype(jnp.bfloat16)
        .reshape(groups, capacity, GROUP_EXPERTS)
    )
    arrived_rows, arrived_gates = (
        lax.all_to_all(send_rows, "sp", split_axis=0, concat_axis=0, tiled=True),
        lax.all_to_all(send_gates, "sp", split_axis=0, concat_axis=0, tiled=True),
    )
    pooled_rows, pooled_gates = (
        lax.all_gather(arrived_rows, "tp", axis=0, tiled=True),
        lax.all_gather(arrived_gates, "tp", axis=0, tiled=True),
    )
    flat_rows = pooled_rows.reshape(-1, width)
    flat_gates = pooled_gates.reshape(-1, GROUP_EXPERTS).astype(jnp.float32)
    gate_pre = jnp.einsum("md,edh->meh", flat_rows, gate_weight, preferred_element_type=jnp.float32)
    up_pre = jnp.einsum("md,edh->meh", flat_rows, up_weight, preferred_element_type=jnp.float32)
    hidden = (jax.nn.silu(gate_pre) * up_pre * flat_gates[:, :, None]).astype(jnp.bfloat16)
    partial_out = jnp.einsum("meh,ehd->md", hidden, down_weight, preferred_element_type=jnp.float32)
    summed = lax.psum_scatter(
        partial_out.reshape(pooled_rows.shape).astype(jnp.bfloat16),
        "tp",
        scatter_dimension=0,
        tiled=True,
    )
    returned = lax.all_to_all(summed, "sp", split_axis=0, concat_axis=0, tiled=True)
    expert_out = lax.dot_general(
        placing,
        returned.reshape(groups * capacity, width),
        (((0,), (0,)), ((), ())),
        preferred_element_type=jnp.float32,
    )
    return (mixed_float + expert_out).astype(jnp.bfloat16)


def solution(mesh):
    placed = (
        P("sp", "tp"),
        P("sp", None),
        P("sp", None),
        P("tp"),
        P("tp", None),
        P(("sp", "tp"), None),
        P(),
        P(),
        P(("sp", "tp")),
        P(("sp", "tp"), None),
        P(("sp", "tp"), None),
        P("sp", None, "tp"),
        P("sp", None, "tp"),
        P("sp", "tp", None),
    )
    return jax.shard_map(
        per_device, mesh=mesh, in_specs=placed, out_specs=P(("sp", "tp"), None), check_vma=False
    )
```

profile of v0, /device:TPU:0, one launch (start us, length us, event | category | flops | bytes accessed | tf_op | source)
XLA Modules:
  0.0 256.5 jit_solution(17460790023405655798)
XLA Ops:
  6.5 1.2 dynamic-slice_bitcast_fusion
  7.8 0.7 copy-done.2
  8.5 0.6 pad_maximum_fusion.3
  9.1 4.9 %collective-permute-start = (bf16[2,128,128]{2,1,0:T(8,128)(2,1)}, bf16[2,128,128]{2,1,0:T(8,128)(2,1)S(1)}, u32[]{:S(2)}, u32[]{:S(2)}) collective-permute-start(bf16[2,128,128]{2,1,0:T(8,128)(2,1)} %get-tuple-element.10), channel_id=1, source_target_pairs={{0,8},{8,16},{16,24},{1,9},{9,17},{17,25},{2,10},{10,18},{18,26},{... | collective-permute-start | bytes 196616 | tf_op jit(solution)/shard_map/ppermute | solution.py:21
  14.0 1.3 collective-permute-start.1
  15.3 0.1 fusion.29
  15.4 0.1 add_add_fusion
  15.5 3.0 %fusion.6 = pred[8,128,384]{1,2,0:T(8,128)(4,1)} fusion(s32[8,384]{1,0:T(8,128)S(1)} %add_add_fusion, s32[8,128]{1,0:T(8,128)S(1)} %add_add_fusion.1, pred[8,384]{1,0:T(8,128)(4,1)S(1)} %get-tuple-element.13, pred[8,384]{1,0:T(8,128)(4,1)S(1)} %get-tuple-element.12), kind=kLoop, calls=%fused_computation.18 | loop fusion | flops 1966080 | bytes 415744 | tf_op jit(solution)/shard_map/and | solution.py:53
  18.5 2.0 reshape.151
  20.4 1.0 pad_maximum_fusion.1
  21.5 0.4 fusion.36
  21.9 0.1 pad_maximum_fusion
  22.0 0.5 copy-done.3
  22.5 0.2 copy-done.5
  22.7 0.6 fusion.4
  23.3 0.0 copy-done.9
  23.3 0.1 broadcast_maximum_fusion
  23.4 0.7 fusion.2
  24.1 0.1 exponential_add_fusion
  24.2 1.1 fusion.9
  25.3 0.3 copy.50
  25.7 3.2 %convolution_convert_fusion = bf16[1024,2048]{1,0:T(8,128)(2,1)} fusion(bf16[256,2048]{1,0:T(8,128)(2,1)S(1)} %copy-done.4, bf16[32,8,8,128]{3,2,1,0:T(8,128)(2,1)S(1)} %bitcast.64), kind=kOutput, calls=%fused_computation.3 | convolution fusion | flops 1075838976 | bytes 5767168 | tf_op jit(solution)/shard_map/dot_general | solution.py:93
  28.9 0.0 reduce-scatter.3.cloned.1.call-update
  28.9 0.0 all-gather.2.cloned.1.call-start
  29.0 0.6 copy-done.8
  29.5 0.1 fusion.24
  29.6 0.2 reduce_window_sum.11
  29.8 0.2 select_reduce_fusion
  30.0 52.0 %reduce-scatter.3.cloned.1.call-done = bf16[128,2048]{1,0:T(8,128)(2,1)} async-done(((bf16[1024,2048]{1,0:T(8,128)(2,1)}), bf16[128,2048]{1,0:T(8,128)(2,1)}) %reduce-scatter.3.cloned.1.call-update) | async-done | bytes 524304 | tf_op jit(solution)/shard_map/reduce_scatter | solution.py:92
  82.0 1.2 fusion.10
  83.2 1.6 fusion.14
  84.8 0.8 copy-done.1
  85.6 0.4 convolution_convert_fusion.1
  86.0 11.6 %all_to_all.15 = bf16[4,40,2048]{2,1,0:T(8,128)(2,1)} all-to-all(bf16[4,40,2048]{2,1,0:T(8,128)(2,1)S(1)} %bitcast.66), channel_id=1, replica_groups=mesh['sp'=4,'tp'=8] {'sp'}, dimensions={0} | all-to-all | bytes 1310720 | tf_op jit(solution)/shard_map/all_to_all | solution.py:131
  97.7 0.0 all-gather.2.cloned.1.call-update
  97.7 0.0 reduce-scatter.5.cloned.1.call-start
  97.8 0.1 convolution_convert_fusion.2
  97.9 0.1 reshape.155
  98.0 7.0 %all_to_all.16 = bf16[4,40,3]{1,2,0:T(4,128)(2,1)S(1)} all-to-all(bf16[4,40,3]{1,2,0:T(4,128)(2,1)S(1)} %copy.51), channel_id=1, replica_groups=mesh['sp'=4,'tp'=8] {'sp'}, dimensions={0} | all-to-all | bytes 1920 | tf_op jit(solution)/shard_map/all_to_all | solution.py:132
  105.1 15.2 %all_gather.7 = bf16[32,40,3]{1,2,0:T(4,128)(2,1)S(1)} all-gather(bf16[4,40,3]{1,2,0:T(4,128)(2,1)S(1)} %all_to_all.16), channel_id=1, replica_groups=mesh['sp'=4,'tp'=8] {'tp'}, dimensions={0}, use_global_device_ids=true | all-gather | bytes 8640 | tf_op jit(solution)/shard_map/all_gather | solution.py:136
  120.3 0.1 reshape.157
  120.4 32.6 %all-gather.2.cloned.1.call-done = bf16[32,40,2048]{2,1,0:T(8,128)(2,1)} async-done(((bf16[4,40,2048]{2,1,0:T(8,128)(2,1)}), bf16[32,40,2048]{2,1,0:T(8,128)(2,1)}) %all-gather.2.cloned.1.call-update) | async-done | bytes 5242896 | tf_op jit(solution)/shard_map/all_gather | solution.py:135
  152.9 9.7 %fusion.37 = f32[1280,3,256]{2,0,1:T(8,128)} fusion(bf16[1280,2048,1]{1,0,2:T(8,128)(2,1)} %bitcast.67, bf16[3,2048,256]{2,1,0:T(8,128)(2,1)} %param.25), kind=kOutput, calls=%fused_computation.70 | convolution fusion | flops 4026531840 | bytes 12320768 | tf_op jit(solution)/shard_map/md,edh->meh/dot_general | solution.py:140
  162.6 14.6 %bitcast_convert_fusion = bf16[1280,2048]{1,0:T(8,128)(2,1)} fusion(bf16[3,256,2048]{2,1,0:T(8,128)(2,1)S(1)} %copy-done, bf16[1280,2048,1]{1,0,2:T(8,128)(2,1)} %bitcast.68, bf16[3,2048,256]{2,1,0:T(8,128)(2,1)} %param.26, f32[1280,3,256]{2,0,1:T(8,128)} %fusion.37, f32[1280,3]{0,1:T(4,128)S(1)} %reshape.157), kind=kOutput, calls=%fused_computation | convolution fusion | flops 8062566400 | bytes 20724736 | tf_op jit(solution)/shard_map/meh,ehd->md/dot_general | solution.py:143
  177.2 0.0 reduce-scatter.5.cloned.1.call-update
  177.2 58.7 %reduce-scatter.5.cloned.1.call-done = bf16[4,40,2048]{2,1,0:T(8,128)(2,1)} async-done(((bf16[32,40,2048]{2,1,0:T(8,128)(2,1)}), bf16[4,40,2048]{2,1,0:T(8,128)(2,1)}) %reduce-scatter.5.cloned.1.call-update) | async-done | bytes 655376 | tf_op jit(solution)/shard_map/reduce_scatter | solution.py:144
  236.0 11.8 %all_to_all.17 = bf16[4,40,2048]{2,1,0:T(8,128)(2,1)S(1)} all-to-all(bf16[4,40,2048]{2,1,0:T(8,128)(2,1)} %reduce-scatter.5.cloned.1.call-done), channel_id=1, replica_groups=mesh['sp'=4,'tp'=8] {'sp'}, dimensions={0} | all-to-all | bytes 1310720 | tf_op jit(solution)/shard_map/all_to_all | solution.py:150
  247.7 2.2 fusion.3
  (30 shorter events, 0.1 us)
Async XLA Ops:
  6.5 156.1 %copy-start = (bf16[3,256,2048]{2,1,0:T(8,128)(2,1)S(1)}, bf16[3,256,2048]{2,1,0:T(8,128)(2,1)}, u32[]{:S(2)}) copy-start(bf16[3,256,2048]{2,1,0:T(8,128)(2,1)} %param.27) | copy-start | bytes 9437188
  6.5 75.4 %reduce-scatter.3.cloned.1.call-start = ((), (), s32[]{:S(2)}) async-start(), calls=%async_computation.5 | async-start | bytes 4718592 | tf_op jit(solution)/shard_map/reduce_scatter | solution.py:92
  7.8 0.7 copy-start.2
  9.1 11.3 %collective-permute-start = (bf16[2,128,128]{2,1,0:T(8,128)(2,1)}, bf16[2,128,128]{2,1,0:T(8,128)(2,1)S(1)}, u32[]{:S(2)}, u32[]{:S(2)}) collective-permute-start(bf16[2,128,128]{2,1,0:T(8,128)(2,1)} %get-tuple-element.10), channel_id=1, source_target_pairs={{0,8},{8,16},{16,24},{1,9},{9,17},{17,25},{2,10},{10,18},{18,26},{... | collective-permute-start | bytes 196616 | tf_op jit(solution)/shard_map/ppermute | solution.py:21
  14.0 6.5 %collective-permute-start.1 = (bf16[2,128,128]{2,1,0:T(8,128)(2,1)S(1)}, bf16[2,128,128]{2,1,0:T(8,128)(2,1)}, u32[]{:S(2)}, u32[]{:S(2)}) collective-permute-start(bf16[2,128,128]{2,1,0:T(8,128)(2,1)S(1)} %get-tuple-element.11), channel_id=1, source_target_pairs={{8,0},{16,8},{24,16},{9,1},{17,9},{25,17},{10,2},{18,10},{26,18},{... | collective-permute-start | bytes 196616 | tf_op jit(solution)/shard_map/ppermute | solution.py:24
  21.5 1.0 copy-start.3
  21.5 1.2 copy-start.5
  22.6 0.7 copy-start.9
  24.2 1.4 copy-start.4
  28.9 0.7 copy-start.8
  28.9 54.3 %copy-start.6 = (f32[2048]{0:T(1024)S(1)}, f32[2048]{0:T(1024)}, u32[]{:S(2)}) copy-start(f32[2048]{0:T(1024)} %param.20) | copy-start | bytes 24580
  28.9 56.7 %copy-start.7 = (f32[2048]{0:T(1024)S(1)}, f32[2048]{0:T(1024)}, u32[]{:S(2)}) copy-start(f32[2048]{0:T(1024)} %param.21) | copy-start | bytes 24580
  28.9 68.8 %copy-start.11 = (bf16[128,2]{0,1:T(2,128)(2,1)S(1)}, bf16[128,2]{0,1:T(2,128)(2,1)}, u32[]{:S(2)}) copy-start(bf16[128,2]{0,1:T(2,128)(2,1)} %param.24) | copy-start | bytes 1540
  28.9 68.8 %copy-start.10 = (s32[128,2]{0,1:T(2,128)S(1)}, s32[128,2]{0,1:T(2,128)}, u32[]{:S(2)}) copy-start(s32[128,2]{0,1:T(2,128)} %param.23) | copy-start | bytes 3076
  28.9 124.0 %all-gather.2.cloned.1.call-start = ((), (), s32[]{:S(2)}) async-start(), calls=%async_computation.6 | async-start | bytes 5898240 | tf_op jit(solution)/shard_map/all_gather | solution.py:135
  84.8 0.8 copy-start.1
  97.7 138.3 %reduce-scatter.5.cloned.1.call-start = ((), (), s32[]{:S(2)}) async-start(), calls=%async_computation.7 | async-start | bytes 5898240 | tf_op jit(solution)/shard_map/reduce_scatter | solution.py:144
Sparse Core Ops, SparseCore 0:
  29.0 52.8 reduce-scatter.2
  97.8 55.0 all-gather.1
  177.4 58.5 reduce-scatter.4
where the time goes:
time: 257 us; the launch traced here: 256 us
  waiting for transfers between devices  143 us (56%)
  blocking collectives  45.6 us (18%)
  matrix products  32 us (12%)
  between operations  13.3 us (5%)
  other arithmetic  9.2 us (4%)
  local copies, waits for them, and re-layouts  6.79 us (3%)
  starting transfers between devices  6.24 us (2%)
    reduce_scatter x1, waiting for transfers between devices, per_device(): lax.psum_scatter(partial_out.reshape(pooled_rows.shape).astype(jnp.bfloat...  58.7 us
    reduce_scatter x1, waiting for transfers between devices, per_device(): lax.psum_scatter(jnp.dot(attended, out_weight, preferred_element_type=jnp...  52 us
    all_gather x1, waiting for transfers between devices, per_device(): lax.all_gather(arrived_rows, 'tp', axis=0, tiled=True)  32.6 us
    all_gather x1, blocking collectives, per_device(): lax.all_gather(arrived_gates, 'tp', axis=0, tiled=True)  15.2 us
    dot_general x1, matrix products, per_device(): jnp.einsum('meh,ehd->md', hidden, down_weight, preferred_element_type=jnp...  14.6 us
    all_to_all x1, blocking collectives, per_device(): lax.all_to_all(summed, 'sp', split_axis=0, concat_axis=0, tiled=True)  11.8 us
    all_to_all x1, blocking collectives, per_device(): lax.all_to_all(send_rows, 'sp', split_axis=0, concat_axis=0, tiled=True)  11.6 us
    dot_general x1, matrix products, per_device(): jnp.einsum('md,edh->meh', flat_rows, gate_weight, preferred_element_type=...  9.71 us
  transfers between devices with their start and end apart: 5, of which 3 were waited for; matrix products, arithmetic and copies ran while one was open for 2% of the time, Pallas kernels for 0%

commit v1 on v0

--- a/solution.py
+++ b/solution.py
@@ -132,7 +132,9 @@
         lax.all_to_all(send_gates, "sp", split_axis=0, concat_axis=0, tiled=True),
     )
     pooled_rows, pooled_gates = (
-        lax.all_gather(arrived_rows, "tp", axis=0, tiled=True),
+        jnp.concatenate(
+            lax.all_to_all(jnp.stack([arrived_rows] * lax.axis_size("tp")), "tp", 0, 0), axis=0
+        ),
         lax.all_gather(arrived_gates, "tp", axis=0, tiled=True),
     )
     flat_rows = pooled_rows.reshape(-1, width)

time: 257 us -> 333 us (1.30)
  blocking collectives: 45.6 us -> 146 us
  waiting for transfers between devices: 143 us -> 104 us
  starting transfers between devices: 6.24 us -> 16.3 us
  local copies, waits for them, and re-layouts: 6.79 us -> 10.4 us
    all_gather x1, blocking collectives: 15.2 us -> 122 us  [per_device(): lax.all_gather(arrived_gates, 'tp', axis=0, tiled=True)]
    all_gather x1 -> x0, waiting for transfers between devices: 32.6 us -> none  [per_device(): lax.all_gather(arrived_rows, 'tp', axis=0, tiled=True)]
    all_to_all x0 -> x2, starting transfers between devices: none -> 10.1 us  [the longest x1 5.46 us: per_device(): lax.all_to_all(send_gates, 'sp', split_axis=0, concat_axis=0, tiled=True)]
    all_to_all x1 -> x0, blocking collectives: 7.03 us -> none  [per_device(): lax.all_to_all(send_gates, 'sp', split_axis=0, concat_axis=0, tiled=True)]
    reduce_scatter x1, waiting for transfers between devices: 52 us -> 45.6 us  [per_device(): lax.psum_scatter(jnp.dot(attended, out_weight, preferred_element_type=jnp...]
  transfers between devices with their start and end apart: 5 -> 6, of which waited for: 3 -> 2; matrix products, arithmetic and copies ran while one was open for 2% -> 3% of each run, Pallas kernels for 0% -> 0%
where the time goes in v1:
time: 333 us
  blocking collectives  146 us (44%)
  waiting for transfers between devices  104 us (31%)
  matrix products  32.8 us (10%)
  starting transfers between devices  16.3 us (5%)
  between operations  13.6 us (4%)
  local copies, waits for them, and re-layouts  10.4 us (3%)
  other arithmetic  9.2 us (3%)
    all_gather x1, blocking collectives, per_device(): lax.all_gather(arrived_gates, 'tp', axis=0, tiled=True)  122 us
    reduce_scatter x1, waiting for transfers between devices, per_device(): lax.psum_scatter(partial_out.reshape(pooled_rows.shape).astype(jnp.bfloat...  58.7 us
    reduce_scatter x1, waiting for transfers between devices, per_device(): lax.psum_scatter(jnp.dot(attended, out_weight, preferred_element_type=jnp...  45.6 us
    dot_general x1, matrix products, per_device(): jnp.einsum('meh,ehd->md', hidden, down_weight, preferred_element_type=jnp...  14.6 us
    all_to_all x1, blocking collectives, per_device(): lax.all_to_all(summed, 'sp', split_axis=0, concat_axis=0, tiled=True)  11.8 us
    all_to_all x1, blocking collectives, per_device(): lax.all_to_all(send_rows, 'sp', split_axis=0, concat_axis=0, tiled=True)  11.8 us
    dot_general x1, matrix products, per_device(): jnp.einsum('md,edh->meh', flat_rows, gate_weight, preferred_element_type=...  9.71 us
  transfers between devices with their start and end apart: 6, of which 2 were waited for; matrix products, arithmetic and copies ran while one was open for 3% of the time, Pallas kernels for 0%

profile of v1, /device:TPU:0, one launch (start us, length us, event | category | flops | bytes accessed | tf_op | source)
XLA Modules:
  0.0 332.7 jit_solution(15827987099144155774)
XLA Ops:
  6.5 1.2 dynamic-slice_bitcast_fusion
  7.8 0.7 copy-done.2
  8.5 0.6 pad_maximum_fusion.3
  9.1 4.9 %collective-permute-start = (bf16[2,128,128]{2,1,0:T(8,128)(2,1)}, bf16[2,128,128]{2,1,0:T(8,128)(2,1)S(1)}, u32[]{:S(2)}, u32[]{:S(2)}) collective-permute-start(bf16[2,128,128]{2,1,0:T(8,128)(2,1)} %get-tuple-element.10), channel_id=1, source_target_pairs={{0,8},{8,16},{16,24},{1,9},{9,17},{17,25},{2,10},{10,18},{18,26},{... | collective-permute-start | bytes 196616 | tf_op jit(solution)/shard_map/ppermute | solution.py:21
  14.0 1.3 collective-permute-start.1
  15.3 0.1 fusion.29
  15.4 0.1 add_add_fusion
  15.4 3.0 fusion.6
  18.5 2.0 reshape.150
  20.4 1.0 pad_maximum_fusion.1
  21.5 0.4 fusion.36
  21.9 0.1 pad_maximum_fusion
  22.0 0.5 copy-done.3
  22.5 0.2 copy-done.5
  22.6 0.6 fusion.4
  23.3 0.0 copy-done.9
  23.3 0.1 broadcast_maximum_fusion
  23.4 0.7 fusion.2
  24.1 0.1 exponential_add_fusion
  24.2 1.1 fusion.9
  25.3 0.3 copy.50
  25.7 3.2 convolution_convert_fusion
  28.9 0.0 reduce-scatter.3.cloned.1.call-update
  28.9 0.6 copy-done.11
  29.6 0.1 fusion.24
  29.6 0.2 reduce_window_sum.11
  29.8 0.2 select_reduce_fusion
  30.0 0.1 convolution_convert_fusion.2
  30.2 0.1 reshape.153
  30.3 0.6 copy.51
  30.9 5.5 %all-to-all-start.2 = ((bf16[4,40,3]{1,2,0:T(4,128)(2,1)}), bf16[4,40,3]{1,2,0:T(4,128)(2,1)S(1)}, u32[]{:S(2)}, u32[]{:S(2)}) async-start(bf16[4,40,3]{1,2,0:T(4,128)(2,1)} %copy.51), calls=%async_computation.3 | async-start | bytes 8192 | tf_op jit(solution)/shard_map/all_to_all | solution.py:132
  36.3 45.6 %reduce-scatter.3.cloned.1.call-done = bf16[128,2048]{1,0:T(8,128)(2,1)} async-done(((bf16[1024,2048]{1,0:T(8,128)(2,1)}), bf16[128,2048]{1,0:T(8,128)(2,1)}) %reduce-scatter.3.cloned.1.call-update) | async-done | bytes 524304 | tf_op jit(solution)/shard_map/reduce_scatter | solution.py:92
  82.0 1.2 fusion.10
  83.2 1.6 fusion.14
  84.9 0.8 copy-done.1
  85.6 1.2 convolution_convert_fusion.1
  86.9 11.8 %all_to_all.20 = bf16[4,40,2048]{2,1,0:T(8,128)(2,1)S(1)} all-to-all(bf16[4,40,2048]{2,1,0:T(8,128)(2,1)} %bitcast.66), channel_id=1, replica_groups=mesh['sp'=4,'tp'=8] {'sp'}, dimensions={0} | all-to-all | bytes 1310720 | tf_op jit(solution)/shard_map/all_to_all | solution.py:131
  98.7 3.0 stack.11
  101.7 4.6 %all-to-all-start.1 = ((bf16[8,4,40,2048]{3,2,1,0:T(8,128)(2,1)}), bf16[8,4,40,2048]{3,2,1,0:T(8,128)(2,1)}, u32[]{:S(2)}, u32[]{:S(2)}) async-start(bf16[8,4,40,2048]{3,2,1,0:T(8,128)(2,1)} %stack.11), calls=%async_computation.2 | async-start | bytes 10485760 | tf_op jit(solution)/shard_map/all_to_all | solution.py:136
  106.3 0.0 reduce-scatter.5.cloned.1.call-start
  106.4 122.5 %all_gather.3 = bf16[32,40,3]{1,2,0:T(4,128)(2,1)S(1)} all-gather(bf16[4,40,3]{1,2,0:T(4,128)(2,1)S(1)} %all-to-all-done.2), channel_id=1, replica_groups=mesh['sp'=4,'tp'=8] {'tp'}, dimensions={0}, use_global_device_ids=true | all-gather | bytes 8640 | tf_op jit(solution)/shard_map/all_gather | solution.py:138
  228.8 0.1 reshape.155
  228.9 9.7 %fusion.37 = f32[1280,3,256]{2,0,1:T(8,128)} fusion(bf16[1280,2048,1]{1,0,2:T(8,128)(2,1)} %bitcast.12, bf16[3,2048,256]{2,1,0:T(8,128)(2,1)} %param.25), kind=kOutput, calls=%fused_computation.70 | convolution fusion | flops 4026531840 | bytes 12320768 | tf_op jit(solution)/shard_map/md,edh->meh/dot_general | solution.py:142
  238.7 14.6 %bitcast_convert_fusion = bf16[1280,2048]{1,0:T(8,128)(2,1)} fusion(bf16[3,256,2048]{2,1,0:T(8,128)(2,1)S(1)} %copy-done, bf16[1280,2048,1]{1,0,2:T(8,128)(2,1)} %bitcast.12, bf16[3,2048,256]{2,1,0:T(8,128)(2,1)} %param.26, f32[1280,3,256]{2,0,1:T(8,128)} %fusion.37, f32[1280,3]{0,1:T(4,128)S(1)} %reshape.155), kind=kOutput, calls=%fused_computation | convolution fusion | flops 8062566400 | bytes 20724736 | tf_op jit(solution)/shard_map/meh,ehd->md/dot_general | solution.py:145
  253.3 0.0 reduce-scatter.5.cloned.1.call-update
  253.3 58.7 %reduce-scatter.5.cloned.1.call-done = bf16[4,40,2048]{2,1,0:T(8,128)(2,1)} async-done(((bf16[32,40,2048]{2,1,0:T(8,128)(2,1)}), bf16[4,40,2048]{2,1,0:T(8,128)(2,1)}) %reduce-scatter.5.cloned.1.call-update) | async-done | bytes 655376 | tf_op jit(solution)/shard_map/reduce_scatter | solution.py:146
  311.9 11.8 %all_to_all.21 = bf16[4,40,2048]{2,1,0:T(8,128)(2,1)S(1)} all-to-all(bf16[4,40,2048]{2,1,0:T(8,128)(2,1)} %reduce-scatter.5.cloned.1.call-done), channel_id=1, replica_groups=mesh['sp'=4,'tp'=8] {'sp'}, dimensions={0} | all-to-all | bytes 1310720 | tf_op jit(solution)/shard_map/all_to_all | solution.py:152
  323.7 2.2 fusion.3
  (31 shorter events, 0.1 us)
Async XLA Ops:
  6.5 232.1 %copy-start = (bf16[3,256,2048]{2,1,0:T(8,128)(2,1)S(1)}, bf16[3,256,2048]{2,1,0:T(8,128)(2,1)}, u32[]{:S(2)}) copy-start(bf16[3,256,2048]{2,1,0:T(8,128)(2,1)} %param.27) | copy-start | bytes 9437188
  6.5 75.5 %reduce-scatter.3.cloned.1.call-start = ((), (), s32[]{:S(2)}) async-start(), calls=%async_computation.6 | async-start | bytes 4718592 | tf_op jit(solution)/shard_map/reduce_scatter | solution.py:92
  7.8 0.7 copy-start.2
  9.1 11.3 %collective-permute-start = (bf16[2,128,128]{2,1,0:T(8,128)(2,1)}, bf16[2,128,128]{2,1,0:T(8,128)(2,1)S(1)}, u32[]{:S(2)}, u32[]{:S(2)}) collective-permute-start(bf16[2,128,128]{2,1,0:T(8,128)(2,1)} %get-tuple-element.10), channel_id=1, source_target_pairs={{0,8},{8,16},{16,24},{1,9},{9,17},{17,25},{2,10},{10,18},{18,26},{... | collective-permute-start | bytes 196616 | tf_op jit(solution)/shard_map/ppermute | solution.py:21
  14.0 6.5 %collective-permute-start.1 = (bf16[2,128,128]{2,1,0:T(8,128)(2,1)S(1)}, bf16[2,128,128]{2,1,0:T(8,128)(2,1)}, u32[]{:S(2)}, u32[]{:S(2)}) collective-permute-start(bf16[2,128,128]{2,1,0:T(8,128)(2,1)S(1)} %get-tuple-element.11), channel_id=1, source_target_pairs={{8,0},{16,8},{24,16},{9,1},{17,9},{25,17},{10,2},{18,10},{26,18},{... | collective-permute-start | bytes 196616 | tf_op jit(solution)/shard_map/ppermute | solution.py:24
  21.5 1.0 copy-start.3
  21.5 1.2 copy-start.5
  22.6 0.7 copy-start.9
  24.2 1.4 copy-start.4
  28.9 0.7 copy-start.11
  28.9 0.7 copy-start.8
  28.9 0.9 copy-start.10
  28.9 54.3 %copy-start.6 = (f32[2048]{0:T(1024)S(1)}, f32[2048]{0:T(1024)}, u32[]{:S(2)}) copy-start(f32[2048]{0:T(1024)} %param.20) | copy-start | bytes 24580
  28.9 56.7 %copy-start.7 = (f32[2048]{0:T(1024)S(1)}, f32[2048]{0:T(1024)}, u32[]{:S(2)}) copy-start(f32[2048]{0:T(1024)} %param.21) | copy-start | bytes 24580
  30.9 56.0 %all-to-all-start.2 = ((bf16[4,40,3]{1,2,0:T(4,128)(2,1)}), bf16[4,40,3]{1,2,0:T(4,128)(2,1)S(1)}, u32[]{:S(2)}, u32[]{:S(2)}) async-start(bf16[4,40,3]{1,2,0:T(4,128)(2,1)} %copy.51), calls=%async_computation.3 | async-start | bytes 8192 | tf_op jit(solution)/shard_map/all_to_all | solution.py:132
  84.8 0.8 copy-start.1
  101.7 127.3 %all-to-all-start.1 = ((bf16[8,4,40,2048]{3,2,1,0:T(8,128)(2,1)}), bf16[8,4,40,2048]{3,2,1,0:T(8,128)(2,1)}, u32[]{:S(2)}, u32[]{:S(2)}) async-start(bf16[8,4,40,2048]{3,2,1,0:T(8,128)(2,1)} %stack.11), calls=%async_computation.2 | async-start | bytes 10485760 | tf_op jit(solution)/shard_map/all_to_all | solution.py:136
  106.3 205.6 %reduce-scatter.5.cloned.1.call-start = ((), (), s32[]{:S(2)}) async-start(), calls=%async_computation.7 | async-start | bytes 5898240 | tf_op jit(solution)/shard_map/reduce_scatter | solution.py:146
Sparse Core Ops, SparseCore 0:
  29.1 52.8 reduce-scatter.2
  253.4 58.4 reduce-scatter.4
